TPU v7x, 32 devices: a whole 2x2x4 slice. The times are simulated.
32 devices in a mesh: grp: 2 (over y), sp: 4 (over z), tp: 4 (over x, core).
Axes of the slice: x: 2, y: 2, z: 4, core: 2. Of those that a mesh axis runs over, the one named last changes fastest.
Arguments:
- inputs: bfloat16 [2048, 2048], P(('grp', 'sp')), parts along dimension 0, may hold values from -6 to 6
- norm_gain: float32 [2048], replicated, may hold values from 0.1 to 1.9
- da_query_weight: bfloat16 [2048, 1024], P('sp', 'tp'), may hold values from -0.125 to 0.125
- da_key_weight: bfloat16 [2048, 1024], P('sp', 'tp'), may hold values from -0.125 to 0.125
- da_value_weight: bfloat16 [2048, 1024], P('sp', 'tp'), may hold values from -0.125 to 0.125
- sw_query_weight: bfloat16 [2048, 1024], P('sp', 'tp'), may hold values from -0.125 to 0.125
- sw_key_weight: bfloat16 [2048, 512], P('sp', 'tp'), may hold values from -0.125 to 0.125
- sw_value_weight: bfloat16 [2048, 512], P('sp', 'tp'), may hold values from -0.125 to 0.125
- da_query_gain: float32 [64], replicated, may hold values from 0.6 to 30
- da_key_gain: float32 [64], replicated, may hold values from 0.6 to 30
- sw_query_gain: float32 [64], replicated, may hold values from 0.6 to 30
- sw_key_gain: float32 [64], replicated, may hold values from 0.6 to 30
- mix_lambda: float32 [8], P('tp'), may hold values from 0.3 to 0.8
- head_gain: float32 [128], replicated, may hold values from 0.1 to 1.9
- sink_logit: float32 [16], P('tp'), may hold values from 0 to 8
- da_out_weight: bfloat16 [1024, 2048], P('tp'), may hold values from -0.1875 to 0.1875
- sw_out_weight: bfloat16 [1024, 2048], P('tp'), may hold values from -0.1875 to 0.1875
Outputs:
- mixed: bfloat16 [2048, 2048], P(('grp', 'sp')), parts along dimension 0
There are 2 independent parts, one for each index of `grp`. A program takes and returns all parts, laid end to end along the dimension named above; an argument that names none is the same for every part. Nothing has to cross between parts.
All inputs are finite; a program needn't handle non-finite values.
Results may differ from a plain program's by a relative error of at most 0.014.
The roundings to bfloat16 on the way count: a program that leaves them out, or rounds other values in their place, can miss the bound.
Values may be sent and summed in bfloat16 or wider, within the bound.
A program may use at most 64 MiB of HBM per device.

v0:
```python
import jax
import jax.numpy as jnp
from jax import lax
from jax.sharding import PartitionSpec as P

HD = 64
WINDOW = 128


def shifted(value, axis, steps):
    count = lax.axis_size(axis)
    first, last = (max(0, -steps), min(count, count - steps))
    return lax.ppermute(value, axis, [(source, source + steps) for source in range(first, last)])


def rms_norm(values, gain):
    return values * lax.rsqrt(jnp.mean(values * values, axis=-1, keepdims=True) + 1e-06) * gain


def absorb(state, queries, places, keys, values, key_places):
    top, total, summed = state
    scores = jnp.einsum(
        "qhmd,khmd->hmqk", queries, keys, preferred_element_type=jnp.float32
    ) * HD ** (-0.5)
    scores = jnp.where(key_places[None, :] <= places[:, None], scores, -jnp.inf)
    new_top = jnp.maximum(top, jnp.max(scores, axis=-1))
    weights = jnp.exp(scores - new_top[..., None])
    total = jnp.sum(weights, axis=-1)
    summed = jnp.einsum(
        "hmqk,khe->hmqe", weights.astype(jnp.bfloat16), values, preferred_element_type=jnp.float32
    )
    return (new_top, total, summed)


def keep(state, queries, places, keys, values, key_places):
    return state


def diff_attention(queries, places, da_key, da_value, mix_lambda, head_gain):
    rows = queries.shape[0]
    heads = queries.shape[1]
    half = rows // 2
    fresh = (
        jnp.full((heads, 2, half), -1e30, jnp.float32),
        jnp.zeros((heads, 2, half), jnp.float32),
        jnp.zeros((heads, 2, half, 2 * HD), jnp.float32),
    )
    states = (fresh, fresh)
    start = jnp.int32(0)
    keys = lax.all_gather(da_key, "sp", axis=0, tiled=True)
    values = lax.all_gather(da_value, "sp", axis=0, tiled=True)
    key_places = jnp.arange(keys.shape[0], dtype=jnp.int32)
    updated = []
    for section in range(2):
        own_rows = queries[section * half : (section + 1) * half]
        own_places = places[section * half : (section + 1) * half]
        updated.append(
            lax.cond(
                start <= jnp.max(own_places),
                absorb,
                keep,
                states[section],
                own_rows,
                own_places,
                keys,
                values,
                key_places,
            )
        )
    states = tuple(updated)
    blended = []
    for top, total, summed in states:
        maps = summed / total[..., None]
        blended.append(maps[:, 0] - mix_lambda[:, None, None] * maps[:, 1])
    blend = jnp.transpose(jnp.concatenate(blended, axis=1), (1, 0, 2))
    return rms_norm(blend, head_gain).astype(jnp.bfloat16).reshape(rows, heads * 2 * HD)


def window_attention(sw_query, sw_key, sw_value, earlier_key, earlier_value, sink_logit, first):
    rows = sw_query.shape[0]
    sw_heads = sw_query.shape[1]
    kv_heads = sw_key.shape[1]
    groups = sw_heads // kv_heads
    count = rows // WINDOW

    def band(own, earlier_tile):
        tiles = own.reshape(count, WINDOW, kv_heads, HD)
        earlier = jnp.concatenate([earlier_tile[None], tiles[:-1]], axis=0)
        return jnp.concatenate([earlier, tiles], axis=1)

    key_band = band(sw_key, earlier_key)
    value_band = band(sw_value, earlier_value)
    query_tiles = sw_query.reshape(count, WINDOW, kv_heads, groups, HD)
    scores = jnp.einsum(
        "nqhgd,nkhd->nhgqk", query_tiles, key_band, preferred_element_type=jnp.float32
    ) * HD ** (-0.5)
    lag = WINDOW + jnp.arange(WINDOW)[:, None] - jnp.arange(2 * WINDOW)[None, :]
    key_places = (
        first + jnp.arange(count)[:, None] * WINDOW - WINDOW + jnp.arange(2 * WINDOW)[None, :]
    )
    valid = ((lag >= 0) & (lag < WINDOW))[None] & (key_places >= 0)[:, None, :]
    scores = jnp.where(valid[:, None, None], scores, -jnp.inf)
    sink = sink_logit.reshape(kv_heads, groups)[None, :, :, None]
    top = jnp.maximum(jnp.max(scores, axis=-1), sink)
    weights = jnp.exp(scores - top[..., None])
    total = jnp.sum(weights, axis=-1) + jnp.exp(sink - top)
    summed = jnp.einsum(
        "nhgqk,nkhd->nqhgd",
        weights.astype(jnp.bfloat16),
        value_band,
        preferred_element_type=jnp.float32,
    )
    return (
        (summed / jnp.transpose(total, (0, 3, 1, 2))[..., None])
        .astype(jnp.bfloat16)
        .reshape(rows, sw_heads * HD)
    )


def on_device(
    inputs,
    norm_gain,
    da_query_weight,
    da_key_weight,
    da_value_weight,
    sw_query_weight,
    sw_key_weight,
    sw_value_weight,
    da_query_gain,
    da_key_gain,
    sw_query_gain,
    sw_key_gain,
    mix_lambda,
    head_gain,
    sink_logit,
    da_out_weight,
    sw_out_weight,
):
    rows = inputs.shape[0]
    normed = rms_norm(inputs.astype(jnp.float32), norm_gain).astype(jnp.bfloat16)
    pieces = (
        lax.all_gather(da_query_weight, "sp", axis=0, tiled=True),
        lax.all_gather(da_key_weight, "sp", axis=0, tiled=True),
        lax.all_gather(da_value_weight, "sp", axis=0, tiled=True),
        lax.all_gather(sw_query_weight, "sp", axis=0, tiled=True),
        lax.all_gather(sw_key_weight, "sp", axis=0, tiled=True),
        lax.all_gather(sw_value_weight, "sp", axis=0, tiled=True),
    )
    projected = tuple(
        (jnp.dot(normed, piece, preferred_element_type=jnp.float32) for piece in pieces)
    )
    da_heads = da_query_weight.shape[1] // (2 * HD)
    sw_heads = sw_query_weight.shape[1] // HD
    kv_heads = sw_key_weight.shape[1] // HD
    da_query = rms_norm(projected[0].reshape(rows, da_heads, 2, HD), da_query_gain).astype(
        jnp.bfloat16
    )
    da_key = rms_norm(projected[1].reshape(rows, da_heads, 2, HD), da_key_gain).astype(jnp.bfloat16)
    da_value = projected[2].astype(jnp.bfloat16).reshape(rows, da_heads, 2 * HD)
    sw_query = rms_norm(projected[3].reshape(rows, sw_heads, HD), sw_query_gain).astype(
        jnp.bfloat16
    )
    sw_key = rms_norm(projected[4].reshape(rows, kv_heads, HD), sw_key_gain).astype(jnp.bfloat16)
    sw_value = projected[5].astype(jnp.bfloat16).reshape(rows, kv_heads, HD)
    place = lax.axis_index("sp")
    first = place * rows
    earlier_key, earlier_value = shifted(
        (sw_key[rows - WINDOW :], sw_value[rows - WINDOW :]), "sp", 1
    )
    sw_rows = window_attention(
        sw_query, sw_key, sw_value, earlier_key, earlier_value, sink_logit, first
    )
    places = first + jnp.arange(rows, dtype=jnp.int32)
    da_rows = diff_attention(da_query, places, da_key, da_value, mix_lambda, head_gain)
    partial_value = jnp.dot(da_rows, da_out_weight, preferred_element_type=jnp.float32) + jnp.dot(
        sw_rows, sw_out_weight, preferred_element_type=jnp.float32
    )
    return lax.psum(partial_value.astype(jnp.bfloat16), "tp")


def solution(mesh):
    return jax.shard_map(
        on_device,
        mesh=mesh,
        in_specs=(
            P(("grp", "sp"), None),
            P(),
            P("sp", "tp"),
            P("sp", "tp"),
            P("sp", "tp"),
            P("sp", "tp"),
            P("sp", "tp"),
            P("sp", "tp"),
            P(),
            P(),
            P(),
            P(),
            P("tp"),
            P(),
            P("tp"),
            P("tp", None),
            P("tp", None),
        ),
        out_specs=P(("grp", "sp"), None),
        check_vma=False,
    )
```

profile of v0, /device:TPU:1, one launch (start us, length us, event | category | flops | bytes accessed | tf_op | source)
XLA Modules:
  0.0 210.7 jit_solution(5717824083418548665)
XLA Ops:
  6.5 0.7 all-gather.9.cloned.1.call-update
  7.3 0.7 all-gather.7.cloned.1.call-update
  8.8 1.5 fusion.29
  10.4 17.9 %all_gather.30 = bf16[2048,128]{1,0:T(8,128)(2,1)S(1)} all-gather(bf16[512,128]{1,0:T(8,128)(2,1)} %param.27), channel_id=1, replica_groups=mesh['grp'=2,'sp'=4,'tp'=4] {'sp'}, dimensions={0}, use_global_device_ids=true | all-gather | bytes 655360 | tf_op jit(solution)/shard_map/all_gather | solution.py:146
  29.6 2.5 %collective-permute-start.1 = (bf16[128,2,64]{0,2,1:T(8,128)(2,1)}, bf16[128,2,64]{0,2,1:T(8,128)(2,1)S(1)}, u32[]{:S(2)}, u32[]{:S(2)}) collective-permute-start(bf16[128,2,64]{0,2,1:T(8,128)(2,1)} %get-tuple-element.55), channel_id=1, source_target_pairs={{0,4},{4,8},{8,12},{1,5},{5,9},{9,13},{2,6},{6,10},{10,14},{3,7},{... | collective-permute-start | bytes 98312 | tf_op jit(solution)/shard_map/ppermute | solution.py:13
  32.1 18.8 %all_gather.29 = bf16[2048,128]{1,0:T(8,128)(2,1)S(1)} all-gather(bf16[512,128]{1,0:T(8,128)(2,1)S(1)} %copy-done.3), channel_id=1, replica_groups=mesh['grp'=2,'sp'=4,'tp'=4] {'sp'}, dimensions={0}, use_global_device_ids=true | all-gather | bytes 655360 | tf_op jit(solution)/shard_map/all_gather | solution.py:147
  52.1 2.0 collective-permute-start
  54.3 0.7 slice_reduce_fusion.1
  57.5 1.9 convolution_convert_fusion
  59.6 18.0 %all-gather.7.cloned.1.call-done = bf16[2048,256]{1,0:T(8,128)(2,1)} async-done(((bf16[512,256]{1,0:T(8,128)(2,1)}), bf16[2048,256]{1,0:T(8,128)(2,1)}) %all-gather.7.cloned.1.call-update) | async-done | bytes 1048592 | tf_op jit(solution)/shard_map/all_gather | solution.py:143
  77.6 1.9 multiply_reduce_fusion.1
  79.6 15.4 %all_gather.26 = bf16[1024,2,2,64]{0,3,2,1:T(8,128)(2,1)S(1)} all-gather(bf16[256,2,2,64]{0,3,2,1:T(8,128)(2,1)S(1)} %multiply_convert_fusion.1), channel_id=1, replica_groups=mesh['grp'=2,'sp'=4,'tp'=4] {'sp'}, dimensions={0}, use_global_device_ids=true | all-gather | bytes 655360 | tf_op jit(solution)/shard_map/all_gather | solution.py:50
  95.0 15.4 %all-gather.5.cloned.1.call-done = bf16[2048,256]{1,0:T(8,128)(2,1)} async-done(((bf16[512,256]{1,0:T(8,128)(2,1)}), bf16[2048,256]{1,0:T(8,128)(2,1)}) %all-gather.5.cloned.1.call-update) | async-done | bytes 1048592 | tf_op jit(solution)/shard_map/all_gather | solution.py:142
  110.4 1.9 multiply_reduce_fusion.2
  112.3 26.9 %all-gather.11.cloned.1.call-done = bf16[2048,256]{1,0:T(8,128)(2,1)} async-done(((bf16[512,256]{1,0:T(8,128)(2,1)}), bf16[2048,256]{1,0:T(8,128)(2,1)}) %all-gather.11.cloned.1.call-update) | async-done | bytes 1048592 | tf_op jit(solution)/shard_map/all_gather | solution.py:145
  139.2 1.9 bitcast_reduce_fusion
  141.2 12.9 %all_gather.28 = bf16[1024,2,128]{2,0,1:T(8,128)(2,1)S(1)} all-gather(bf16[256,2,128]{2,0,1:T(8,128)(2,1)S(1)} %copy.26), channel_id=1, replica_groups=mesh['grp'=2,'sp'=4,'tp'=4] {'sp'}, dimensions={0}, use_global_device_ids=true | all-gather | bytes 655360 | tf_op jit(solution)/shard_map/all_gather | solution.py:51
  154.2 2.3 %conditional.3 = (f32[2,2,128]{2,1,0:T(2,128)S(1)}, f32[2,2,128,128]{2,3,0,1:T(8,128)S(1)}) conditional(s32[]{:T(128)} %convert_element_type.58, () %tuple.23, (s32[1024]{0:T(1024)S(1)}, s32[128]{0:T(128)S(1)}, bf16[256,2,2,64]{0,3,2,1:T(8,128)(2,1)S(1)}, bf16[1024,2,2,64]{0,3,2,1:T(8,128)(2,1)S(1)}, bf16[1024,2,128]{2,0,1:T(8,128)(2,1)S(1)}) %tuple.24), branch_computations={%region_9.10_spmd, %region_10.13_spmd} | conditional | flops 207224320 | bytes 8733200 | solution.py:58
  155.6 0.7 fusion.17
  156.5 2.3 %conditional.2 = (f32[2,2,128]{2,1,0:T(2,128)S(1)}, f32[2,2,128,128]{2,3,0,1:T(8,128)S(1)}) conditional(s32[]{:T(128)} %convert_element_type.52, () %tuple.21, (s32[1024]{0:T(1024)S(1)}, s32[128]{0:T(128)S(1)}, bf16[256,2,2,64]{0,3,2,1:T(8,128)(2,1)S(1)}, bf16[1024,2,2,64]{0,3,2,1:T(8,128)(2,1)S(1)}, bf16[1024,2,128]{2,0,1:T(8,128)(2,1)S(1)}) %tuple.22), branch_computations={%region_4.0_spmd, %region_5.8_spmd} | conditional | flops 207224320 | bytes 8733200 | solution.py:58
  157.9 0.7 fusion.3
  161.5 1.4 fusion.28
  163.0 38.9 %all-reduce.2.cloned.1.call-done = bf16[256,2048]{1,0:T(8,128)(2,1)} async-done(((bf16[256,2048]{1,0:T(8,128)(2,1)}), bf16[256,2048]{1,0:T(8,128)(2,1)}) %all-reduce.2.cloned.1.call-update) | async-done | bytes 1048592 | tf_op jit(solution)/shard_map/psum | solution.py:178
  201.9 2.3 %copy.73 = bf16[256,2048]{1,0:T(8,128)(2,1)} copy(bf16[256,2048]{1,0:T(8,128)(2,1)} %all-reduce.2.cloned.1.call-done) | data formatting | bytes 2097152
  (92 shorter events, 10.5 us)
Async XLA Ops:
  6.5 154.0 %copy-start = (bf16[256,2048]{1,0:T(8,128)(2,1)S(1)}, bf16[256,2048]{1,0:T(8,128)(2,1)}, u32[]{:S(2)}) copy-start(bf16[256,2048]{1,0:T(8,128)(2,1)} %param.36) | copy-start | bytes 3145732
  6.5 21.7 %copy-start.1 = (bf16[256,2048]{1,0:T(8,128)(2,1)S(1)}, bf16[256,2048]{1,0:T(8,128)(2,1)}, u32[]{:S(2)}) copy-start(bf16[256,2048]{1,0:T(8,128)(2,1)} %param.21) | copy-start | bytes 3145732
  6.5 21.7 %copy-start.12 = (f32[2048]{0:T(1024)S(1)}, f32[2048]{0:T(1024)}, u32[]{:S(2)}) copy-start(f32[2048]{0:T(1024)} %param.22) | copy-start | bytes 24580
  6.5 51.0 %all-gather.9.cloned.1.call-start = ((), (), s32[]{:S(2)}) async-start(), calls=%async_computation.2 | async-start | bytes 1310720 | tf_op jit(solution)/shard_map/all_gather | solution.py:144
  7.3 70.3 %all-gather.7.cloned.1.call-start = ((), (), s32[]{:S(2)}) async-start(), calls=%async_computation.1 | async-start | bytes 1310720 | tf_op jit(solution)/shard_map/all_gather | solution.py:143
  8.0 20.8 %copy-start.7 = (f32[64]{0:T(128)S(1)}, f32[64]{0:T(128)}, u32[]{:S(2)}) copy-start(f32[64]{0:T(128)} %param.32) | copy-start | bytes 772
  8.0 102.4 %all-gather.5.cloned.1.call-start = ((), (), s32[]{:S(2)}) async-start(), calls=%async_computation | async-start | bytes 1310720 | tf_op jit(solution)/shard_map/all_gather | solution.py:142
  8.8 23.4 %copy-start.3 = (bf16[512,128]{1,0:T(8,128)(2,1)S(1)}, bf16[512,128]{1,0:T(8,128)(2,1)}, u32[]{:S(2)}) copy-start(bf16[512,128]{1,0:T(8,128)(2,1)} %param.28) | copy-start | bytes 393220
  8.8 130.5 %all-gather.11.cloned.1.call-start = ((), (), s32[]{:S(2)}) async-start(), calls=%async_computation.3 | async-start | bytes 1310720 | tf_op jit(solution)/shard_map/all_gather | solution.py:145
  28.8 27.7 %copy-start.13 = (f32[4]{0:T(128)S(1)}, f32[4]{0:T(128)}, u32[]{:S(2)}) copy-start(f32[4]{0:T(128)} %param.35) | copy-start | bytes 52
  29.6 129.4 %collective-permute-start.1 = (bf16[128,2,64]{0,2,1:T(8,128)(2,1)}, bf16[128,2,64]{0,2,1:T(8,128)(2,1)S(1)}, u32[]{:S(2)}, u32[]{:S(2)}) collective-permute-start(bf16[128,2,64]{0,2,1:T(8,128)(2,1)} %get-tuple-element.55), channel_id=1, source_target_pairs={{0,4},{4,8},{8,12},{1,5},{5,9},{9,13},{2,6},{6,10},{10,14},{3,7},{... | collective-permute-start | bytes 98312 | tf_op jit(solution)/shard_map/ppermute | solution.py:13
  52.1 107.8 %collective-permute-start = (bf16[128,2,64]{0,2,1:T(8,128)(2,1)}, bf16[128,2,64]{0,2,1:T(8,128)(2,1)S(1)}, u32[]{:S(2)}, u32[]{:S(2)}) collective-permute-start(bf16[128,2,64]{0,2,1:T(8,128)(2,1)} %bitcast.13), channel_id=1, source_target_pairs={{0,4},{4,8},{8,12},{1,5},{5,9},{9,13},{2,6},{6,10},{10,14},{3,7},{... | collective-permute-start | bytes 98312 | tf_op jit(solution)/shard_map/ppermute | solution.py:13
  54.2 147.7 %all-reduce.2.cloned.1.call-start = ((), (), s32[]{:S(2)}) async-start(), calls=%async_computation.4 | async-start | bytes 2097152 | tf_op jit(solution)/shard_map/psum | solution.py:178
  59.4 20.1 %copy-start.8 = (f32[64]{0:T(128)S(1)}, f32[64]{0:T(128)}, u32[]{:S(2)}) copy-start(f32[64]{0:T(128)} %param.30) | copy-start | bytes 772
  112.3 28.8 %copy-start.9 = (f32[64]{0:T(128)S(1)}, f32[64]{0:T(128)}, u32[]{:S(2)}) copy-start(f32[64]{0:T(128)} %param.29) | copy-start | bytes 772
  156.5 2.5 %copy-start.6 = (bf16[1,128,2,64]{1,3,2,0:T(8,128)(2,1)S(1)}, bf16[1,128,2,64]{1,3,2,0:T(8,128)(2,1)}, u32[]{:S(2)}) copy-start(bf16[1,128,2,64]{1,3,2,0:T(8,128)(2,1)} %get-tuple-element.56) | copy-start | bytes 98308
  156.5 2.5 %copy-start.14 = (f32[64]{0:T(128)S(1)}, f32[64]{0:T(128)}, u32[]{:S(2)}) copy-start(f32[64]{0:T(128)} %param.31) | copy-start | bytes 772
  158.8 1.0 copy-start.11
  159.0 1.0 copy-start.4
  159.0 1.0 copy-start.5
  159.7 0.7 copy-start.10
  160.3 1.2 copy-start.2
Sparse Core Ops, SparseCore 0:
  8.9 38.9 all-gather.8
  49.5 28.0 all-gather.6
  79.2 31.1 all-gather.4
  111.8 27.3 all-gather.10
  163.1 38.7 all-reduce.1
where the time goes:
time: 212 us; the launch traced here: 211 us
  waiting for transfers between devices  101 us (48%)
  blocking collectives  65 us (31%)
  between operations  14.9 us (7%)
  matrix products  14 us (7%)
  local copies, waits for them, and re-layouts  5.61 us (3%)
  other arithmetic  5.05 us (2%)
  starting transfers between devices  4.69 us (2%)
    psum x1, waiting for transfers between devices, on_device(): return lax.psum(partial_value.astype(jnp.bfloat16), 'tp')  38.9 us
    all_gather x1, waiting for transfers between devices, on_device(): lax.all_gather(sw_query_weight, 'sp', axis=0, tiled=True)  26.9 us
    all_gather x1, blocking collectives, on_device(): lax.all_gather(sw_value_weight, 'sp', axis=0, tiled=True)  18.8 us
    all_gather x1, waiting for transfers between devices, on_device(): lax.all_gather(da_key_weight, 'sp', axis=0, tiled=True)  18 us
    all_gather x1, blocking collectives, on_device(): lax.all_gather(sw_key_weight, 'sp', axis=0, tiled=True)  17.9 us
    all_gather x1, blocking collectives, diff_attention(): keys = lax.all_gather(da_key, 'sp', axis=0, tiled=True)  15.4 us
    all_gather x1, waiting for transfers between devices, on_device(): lax.all_gather(da_query_weight, 'sp', axis=0, tiled=True)  15.4 us
    all_gather x1, blocking collectives, diff_attention(): values = lax.all_gather(da_value, 'sp', axis=0, tiled=True)  12.9 us
  transfers between devices with their start and end apart: 7, of which 4 were waited for; matrix products, arithmetic and copies ran while one was open for 9% of the time, Pallas kernels for 0%

commit v1 on v0

--- a/solution.py
+++ b/solution.py
@@ -1,6 +1,10 @@
+import functools
+
 import jax
 import jax.numpy as jnp
 from jax import lax
+from jax.experimental import pallas as pl
+from jax.experimental.pallas import tpu as pltpu
 from jax.sharding import PartitionSpec as P
 
 HD = 64
@@ -178,9 +182,528 @@
     return lax.psum(partial_value.astype(jnp.bfloat16), "tp")
 
 
+MESH = pl.DeviceIdType.MESH
+F32, BF16 = jnp.float32, jnp.bfloat16
+CORES = 2
+
+
+def dot(a, b):
+    return jnp.dot(a, b, preferred_element_type=F32)
+
+
+def dot_t(a, b):
+    return lax.dot_general(a, b, (((1,), (1,)), ((), ())), preferred_element_type=F32)
+
+
+def pair_norm(values, gain):
+    lane = lax.broadcasted_iota(jnp.int32, values.shape, 1)
+    squares = values * values
+    low = jnp.sum(jnp.where(lane < HD, squares, 0.0), axis=-1, keepdims=True)
+    high = jnp.sum(jnp.where(lane < HD, 0.0, squares), axis=-1, keepdims=True)
+    mean = jnp.where(lane < HD, low, high) * (1.0 / HD)
+    return values * lax.rsqrt(mean + 1e-06) * gain
+
+
+def kernel(
+    n,
+    x_ref,
+    w_ref,
+    norm_gain_ref,
+    gains_ref,
+    scalars_ref,
+    da_out_ref,
+    sw_out_ref,
+    out_ref,
+    xg,
+    wb,
+    normed,
+    query,
+    kv,
+    scal,
+    rows_out,
+    rows_in,
+    part_out,
+    part_in,
+    sum_out,
+    sum_in,
+    local_sem,
+    x_send,
+    x_recv,
+    xf_send,
+    xf_recv,
+    w_send,
+    w_recv,
+    wy_send,
+    wy_recv,
+    wc_send,
+    wc_recv,
+    own_send,
+    own_recv,
+    kv_send,
+    kv_recv,
+    sc_send,
+    sc_recv,
+    r_send,
+    r_recv,
+    p_send,
+    p_recv,
+    s_send,
+    s_recv,
+    o_send,
+    o_recv,
+):
+    y = lax.axis_index("grp")
+    z = lax.axis_index("sp")
+    t = lax.axis_index("tp")
+    x = t // CORES
+    c = t % CORES
+    peer = {"tp": x * CORES + 1 - c}
+    across = {"tp": (1 - x) * CORES + c}
+    beside = {"grp": 1 - y}
+
+    def at(zz, cc):
+        return {"sp": zz, "tp": x * CORES + cc}
+
+    def remote(src, dst, send, recv, device):
+        return pltpu.make_async_remote_copy(
+            src_ref=src,
+            dst_ref=dst,
+            send_sem=send,
+            recv_sem=recv,
+            device_id=device,
+            device_id_type=MESH,
+        )
+
+    barrier = pltpu.get_barrier_semaphore()
+
+    def greet(device):
+        pl.semaphore_signal(barrier, inc=1, device_id=device, device_id_type=MESH)
+
+    greet(peer)
+    greet(across)
+    greet(beside)
+    for k in range(1, n):
+        for cc in range(CORES):
+            greet(at(lax.rem(z + k, n), cc))
+    pl.semaphore_wait(barrier, 3 + (n - 1) * CORES)
+
+    pending = []
+
+    def go(copy, when=None):
+        if when is None:
+            copy.start()
+        else:
+            pl.when(when)(copy.start)
+        pending.append((copy, when))
+
+    def hop(d, k):
+        source = z - k if d == 0 else z + k
+        source = jnp.clip(source, 0, n - 1)
+        target = jnp.clip(z + 1 if d == 0 else z - 1, 0, n - 1)
+        src = x_ref.at[c, x] if k == 0 else xg.at[source, x]
+        return remote(
+            src, xg.at[source, x], x_send.at[d, k], x_recv.at[d, k], {"sp": target}
+        )
+
+    def can_hop(d, k):
+        return (z - k >= 0) & (z + 1 < n) if d == 0 else (z + k < n) & (z >= 1)
+
+    def has(d, k):
+        return z - k >= 0 if d == 0 else z + k < n
+
+    go(hop(0, 0), can_hop(0, 0))
+    go(hop(1, 0), can_hop(1, 0))
+
+    for par in range(CORES):
+        zt = CORES * c + par
+        for cd in range(CORES):
+            go(
+                remote(
+                    w_ref.at[par, y, cd],
+                    wb.at[z, y, cd],
+                    w_send.at[par, cd],
+                    w_recv.at[z],
+                    at(zt, cd),
+                ),
+                zt != z,
+            )
+    owner = c == z // CORES
+    own = remote(w_ref.at[z % CORES], wb.at[z], own_send, own_recv, peer)
+    go(own, owner)
+    own_local = pltpu.make_async_copy(w_ref.at[z % CORES], wb.at[z], local_sem.at[0])
+    pl.when(owner)(own_local.start)
+    own_x = pltpu.make_async_copy(x_ref.at[c], xg.at[z], local_sem.at[1])
+    own_x.start()
+    sc_local = pltpu.make_async_copy(scalars_ref, scal.at[c], local_sem.at[2])
+    sc_local.start()
+    sc = remote(scalars_ref, scal.at[c], sc_send, sc_recv, peer)
+    go(sc)
+
+    def cross(zs):
+        return remote(xg.at[zs, x], xg.at[zs, x], xf_send.at[zs], xf_recv.at[zs], across)
+
+    def weight_direct(zs):
+        return remote(wb.at[zs, y, c], wb.at[zs, y, c], w_send.at[0, 0], w_recv.at[zs], peer)
+
+    def weight_beside(zs):
+        return remote(wb.at[zs, y, c], wb.at[zs, y, c], wy_send.at[zs], wy_recv.at[zs], beside)
+
+    def weight_core(zs, which):
+        yy = y if which == 0 else 1 - y
+        return remote(
+            wb.at[zs, yy, c], wb.at[zs, yy, c], wc_send.at[which, zs], wc_recv.at[which, zs], peer
+        )
+
+    for k in range(1, n):
+        for d in range(2):
+            there = has(d, k)
+            zs = jnp.clip(z - k if d == 0 else z + k, 0, n - 1)
+
+            def arrived(zs=zs, d=d, k=k):
+                remote(
+                    xg.at[zs, x], xg.at[zs, x], x_send.at[d, k - 1], x_recv.at[d, k - 1], across
+                ).wait_recv()
+
+            pl.when(there)(arrived)
+            if k < n - 1:
+                go(hop(d, k), can_hop(d, k))
+            go(cross(zs), there)
+        for d in range(2):
+            there = has(d, k)
+            zs = jnp.clip(z - k if d == 0 else z + k, 0, n - 1)
+            pl.when(there)(lambda zs=zs: weight_direct(zs).wait_recv())
+            go(weight_beside(zs), there)
+            go(weight_core(zs, 0), there)
+    others = [lax.rem(z + k, n) for k in range(1, n)]
+    for zs in others:
+        remote(wb.at[zs, 1 - y, c], wb.at[zs, 1 - y, c], wy_send.at[zs], wy_recv.at[zs], beside).wait_recv()
+        go(weight_core(zs, 1))
+    for zs in others:
+        remote(
+            xg.at[zs, 1 - x], xg.at[zs, 1 - x], xf_send.at[zs], xf_recv.at[zs], across
+        ).wait_recv()
+    own_x.wait()
+
+    part = xg.shape[2]
+    tile = 2 * part
+    for i in range(n):
+        for h in range(2):
+            values = xg[i, h].astype(F32)
+            values = rms_norm(values, norm_gain_ref[...])
+            normed[i, h * part : (h + 1) * part, :] = values.astype(BF16)
+
+    pl.when(owner)(own_local.wait)
+    pl.when(jnp.logical_not(owner))(own.wait_recv)
+    for zs in others:
+        for which in range(2):
+            yy = y if which == 0 else 1 - y
+            remote(
+                wb.at[zs, yy, 1 - c],
+                wb.at[zs, yy, 1 - c],
+                wc_send.at[which, zs],
+                wc_recv.at[which, zs],
+                peer,
+            ).wait_recv()
+
+    depth = wb.shape[1] * wb.shape[2] * wb.shape[3]
+    wide = 2 * HD
+    width = wb.shape[4]
+    for i in range(n):
+        acc = dot(normed[i, :, 0:depth], wb[0].reshape(depth, width))
+        for j in range(1, n):
+            acc += dot(normed[i, :, j * depth : (j + 1) * depth], wb[j].reshape(depth, width))
+        da_q = pair_norm(acc[:, 0:wide], gains_ref[0:1, :]).astype(BF16)
+        da_k = pair_norm(acc[:, wide : 2 * wide], gains_ref[1:2, :]).astype(BF16)
+        da_v = acc[:, 2 * wide : 3 * wide].astype(BF16)
+        sw_q = pair_norm(acc[:, 3 * wide : 4 * wide], gains_ref[2:3, :]).astype(BF16)
+        sw_kv = acc[:, 4 * wide : 5 * wide]
+        lane = lax.broadcasted_iota(jnp.int32, sw_kv.shape, 1)
+        sw_kv = jnp.where(lane < HD, pair_norm(sw_kv, gains_ref[3:4, :]), sw_kv).astype(BF16)
+        scale = jnp.asarray(HD ** (-0.5), BF16)
+        query[i, :, 0:wide] = da_q * scale
+        query[i, :, wide : 2 * wide] = sw_q * scale
+        kv[c, i, :, 0:wide] = da_k
+        kv[c, i, :, wide : 2 * wide] = da_v
+        kv[c, i, :, 2 * wide : 3 * wide] = sw_kv
+
+    swap = remote(kv.at[c], kv.at[c], kv_send, kv_recv, peer)
+    go(swap)
+    sc_local.wait()
+    remote(scal.at[1 - c], scal.at[1 - c], sc_send, sc_recv, peer).wait_recv()
+    remote(kv.at[1 - c], kv.at[1 - c], kv_send, kv_recv, peer).wait_recv()
+
+    mine = scal[z // CORES, z % CORES]
+    mix = mine[0:1, :]
+    for i in range(n):
+        q_place = (2 * i + c) * tile + lax.broadcasted_iota(jnp.int32, (tile, 1), 0)
+        count = (i + 1) * tile
+        column = lax.broadcasted_iota(jnp.int32, (1, count), 1)
+        maps = []
+        for m in range(2):
+            q = query[i, :, m * HD : (m + 1) * HD]
+            scores = []
+            for h in range(2):
+                keys = kv[h, 0 : i + 1, :, m * HD : (m + 1) * HD].reshape(count, HD)
+                place = (column // tile) * (2 * tile) + h * tile + column % tile
+                scores.append(jnp.where(place <= q_place, dot_t(q, keys), -jnp.inf))
+            top = jnp.maximum(
+                jnp.max(scores[0], axis=-1, keepdims=True),
+                jnp.max(scores[1], axis=-1, keepdims=True),
+            )
+            total = 0.0
+            summed = 0.0
+            for h in range(2):
+                weights = jnp.exp(scores[h] - top)
+                total += jnp.sum(weights, axis=-1, keepdims=True)
+                values = kv[h, 0 : i + 1, :, wide : 2 * wide].reshape(count, wide)
+                summed += dot(weights.astype(BF16), values)
+            maps.append(summed / total)
+        blend = maps[0] - mix * maps[1]
+        rows_out[i, :, 0:wide] = rms_norm(blend, gains_ref[4:5, :]).astype(BF16)
+
+        before = jnp.maximum(i - 1 + c, 0)
+        q_row = lax.broadcasted_iota(jnp.int32, (tile, tile), 0)
+        k_row = lax.broadcasted_iota(jnp.int32, (tile, tile), 1)
+        first_ok = (2 * i + c) > 0
+        near = kv[c, i, :, 2 * wide : 3 * wide]
+        far = kv[1 - c, before, :, 2 * wide : 3 * wide]
+        results = []
+        for g in range(2):
+            q = query[i, :, wide + g * HD : wide + (g + 1) * HD]
+            s_near = jnp.where(k_row <= q_row, dot_t(q, near[:, 0:HD]), -jnp.inf)
+            s_far = jnp.where((k_row > q_row) & first_ok, dot_t(q, far[:, 0:HD]), -jnp.inf)
+            sink = mine[1 + g : 2 + g, 0:1]
+            top = jnp.maximum(
+                jnp.max(s_near, axis=-1, keepdims=True), jnp.max(s_far, axis=-1, keepdims=True)
+            )
+            top = jnp.maximum(top, sink)
+            w_near = jnp.exp(s_near - top)
+            w_far = jnp.exp(s_far - top)
+            total = (
+                jnp.sum(w_near, axis=-1, keepdims=True)
+                + jnp.sum(w_far, axis=-1, keepdims=True)
+                + jnp.exp(sink - top)
+            )
+            summed = dot(w_near.astype(BF16), near[:, HD:wide]) + dot(
+                w_far.astype(BF16), far[:, HD:wide]
+            )
+            results.append(summed / total)
+        rows_out[i, :, wide : 2 * wide] = jnp.concatenate(results, axis=-1).astype(BF16)
+
+        away = (z != i) | jnp.logical_not(owner)
+        go(
+            remote(
+                rows_out.at[i],
+                rows_in.at[z % CORES, c],
+                r_send.at[i],
+                r_recv.at[z % CORES, c],
+                at(i, z // CORES),
+            ),
+            away,
+        )
+    keep_rows = pltpu.make_async_copy(rows_out.at[z], rows_in.at[z % CORES, c], local_sem.at[3])
+    pl.when(owner)(keep_rows.start)
+    pl.when(owner)(keep_rows.wait)
+
+    def await_rows(cc):
+        for par in range(CORES):
+
+            def wait(par=par):
+                remote(
+                    rows_in.at[par, cc], rows_in.at[par, cc], r_send.at[0], r_recv.at[par, cc], peer
+                ).wait_recv()
+
+            pl.when((CORES * c + par != z) | (cc != c))(wait)
+
+    columns = part_out.shape[1] // 4
+
+    def project(cc, q):
+        cols = slice(q * columns, (q + 1) * columns)
+        acc = 0.0
+        for par in range(CORES):
+            rows = rows_in[par, cc]
+            acc += dot(rows[:, 0:wide], da_out_ref[par * wide : (par + 1) * wide, cols])
+            acc += dot(rows[:, wide : 2 * wide], sw_out_ref[par * wide : (par + 1) * wide, cols])
+        return acc.astype(BF16)
+
+    await_rows(1 - c)
+    for q in range(4):
+        part_out[:, q * columns : (q + 1) * columns] = project(1 - c, q)
+        cols = pl.ds(q * columns, columns)
+        go(remote(part_out.at[:, cols], part_in.at[:, cols], p_send.at[q], p_recv.at[q], peer))
+    await_rows(c)
+    for q in range(4):
+        cols = pl.ds(q * columns, columns)
+        mine_part = project(c, q).astype(F32)
+        remote(part_out.at[:, cols], part_in.at[:, cols], p_send.at[q], p_recv.at[q], peer).wait_recv()
+        both = mine_part + part_in[:, cols].astype(F32)
+        sum_out[:, cols] = both.astype(BF16)
+        go(remote(sum_out.at[:, cols], sum_in.at[:, cols], s_send.at[q], s_recv.at[q], across))
+    for q in range(4):
+        cols = pl.ds(q * columns, columns)
+        remote(sum_out.at[:, cols], sum_in.at[:, cols], s_send.at[q], s_recv.at[q], across).wait_recv()
+        total = sum_out[:, cols].astype(F32) + sum_in[:, cols].astype(F32)
+        out_ref[c, :, cols] = total.astype(BF16)
+        go(
+            remote(
+                out_ref.at[c, :, cols], out_ref.at[c, :, cols], o_send.at[q], o_recv.at[q], peer
+            )
+        )
+    for q in range(4):
+        cols = pl.ds(q * columns, columns)
+        remote(
+            out_ref.at[1 - c, :, cols], out_ref.at[1 - c, :, cols], o_send.at[q], o_recv.at[q], peer
+        ).wait_recv()
+    for copy, when in pending:
+        if when is None:
+            copy.wait_send()
+        else:
+            pl.when(when)(copy.wait_send)
+
+
+def transposed(n, *arrays):
+    (
+        inputs,
+        norm_gain,
+        da_query_weight,
+        da_key_weight,
+        da_value_weight,
+        sw_query_weight,
+        sw_key_weight,
+        sw_value_weight,
+        da_query_gain,
+        da_key_gain,
+        sw_query_gain,
+        sw_key_gain,
+        mix_lambda,
+        head_gain,
+        sink_logit,
+        da_out_weight,
+        sw_out_weight,
+    ) = arrays
+    rows, d = inputs.shape
+    depth = da_query_weight.shape[0]
+    wide = 2 * HD
+    packed = []
+    for par in range(CORES):
+        big = slice(par * wide, (par + 1) * wide)
+        small = slice(par * HD, (par + 1) * HD)
+        packed.append(
+            jnp.concatenate(
+                [
+                    da_query_weight[:, big],
+                    da_key_weight[:, big],
+                    da_value_weight[:, big],
+                    sw_query_weight[:, big],
+                    sw_key_weight[:, small],
+                    sw_value_weight[:, small],
+                ],
+                axis=1,
+            )
+        )
+    width = packed[0].shape[1]
+    piece = depth // 4
+    weights = jnp.stack(packed).reshape(CORES, 2, CORES, piece, width)
+    gains = jnp.stack(
+        [
+            jnp.tile(da_query_gain, 2),
+            jnp.tile(da_key_gain, 2),
+            jnp.tile(sw_query_gain, 2),
+            jnp.tile(sw_key_gain, 2),
+            head_gain,
+            head_gain,
+            head_gain,
+            head_gain,
+        ]
+    )
+    sinks = sink_logit.reshape(CORES, 2)
+    scalars = jnp.concatenate([mix_lambda.reshape(CORES, 1), sinks, jnp.zeros((CORES, 5), F32)], axis=1)
+    scalars = jnp.broadcast_to(scalars[:, :, None], (CORES, 8, wide))
+    part = rows // 4
+    tile = rows // 2
+    DMA = pltpu.SemaphoreType.DMA
+    vmem = pl.BlockSpec(memory_space=pltpu.VMEM)
+    out = pl.pallas_call(
+        functools.partial(kernel, n),
+        out_shape=jax.ShapeDtypeStruct((2, tile, d), BF16),
+        in_specs=[vmem] * 7,
+        out_specs=vmem,
+        scratch_shapes=[
+            pltpu.VMEM((n, 2, part, d), BF16),
+            pltpu.VMEM((n, 2, CORES, piece, width), BF16),
+            pltpu.VMEM((n, tile, d), BF16),
+            pltpu.VMEM((n, tile, 2 * wide), BF16),
+            pltpu.VMEM((2, n, tile, 3 * wide), BF16),
+            pltpu.VMEM((CORES, CORES, 8, wide), F32),
+            pltpu.VMEM((n, tile, 2 * wide), BF16),
+            pltpu.VMEM((CORES, CORES, tile, 2 * wide), BF16),
+            pltpu.VMEM((tile, d), BF16),
+            pltpu.VMEM((tile, d), BF16),
+            pltpu.VMEM((tile, d), BF16),
+            pltpu.VMEM((tile, d), BF16),
+            DMA((4,)),
+            DMA((2, n)),
+            DMA((2, n)),
+            DMA((n,)),
+            DMA((n,)),
+            DMA((CORES, CORES)),
+            DMA((n,)),
+            DMA((n,)),
+            DMA((n,)),
+            DMA((2, n)),
+            DMA((2, n)),
+            DMA,
+            DMA,
+            DMA,
+            DMA,
+            DMA,
+            DMA,
+            DMA((n,)),
+            DMA((CORES, CORES)),
+            DMA((4,)),
+            DMA((4,)),
+            DMA((4,)),
+            DMA((4,)),
+            DMA((4,)),
+            DMA((4,)),
+        ],
+        compiler_params=pltpu.CompilerParams(
+            collective_id=0, has_side_effects=True, vmem_limit_bytes=60 * 1024 * 1024
+        ),
+    )(
+        inputs.reshape(CORES, 2, part, d),
+        weights,
+        norm_gain.reshape(1, d),
+        gains,
+        scalars,
+        da_out_weight,
+        sw_out_weight,
+    )
+    return out.reshape(rows, d)
+
+
+def body(sizes, *arrays):
+    rows = arrays[0].shape[0]
+    heads = arrays[12].shape[0]
+    sinks = arrays[14].shape[0]
+    n = sizes["sp"]
+    fits = (
+        sizes["grp"] == 2
+        and sizes["tp"] == 2 * CORES
+        and n == 2 * CORES
+        and heads == CORES
+        and sinks == 2 * CORES
+        and arrays[6].shape[1] == CORES * HD
+        and rows == 2 * WINDOW
+    )
+    if fits:
+        return transposed(n, *arrays)
+    return on_device(*arrays)
+
+
 def solution(mesh):
     return jax.shard_map(
-        on_device,
+        functools.partial(body, dict(mesh.shape)),
         mesh=mesh,
         in_specs=(
             P(("grp", "sp"), None),

time: 212 us -> 83.4 us (0.39)
  waiting for transfers between devices: 101 us -> 0 us
  Pallas kernels: 0 us -> 73 us
  blocking collectives: 65 us -> 0 us
  between operations: 14.9 us -> 0.13 us
  matrix products: 14 us -> 0 us
  starting transfers between devices: 4.69 us -> 0 us
  other arithmetic: 5.05 us -> 1.31 us
    pallas_call x0 -> x1, Pallas kernels: none -> 73 us  [transposed(): pl.pallas_call(functools.partial(kernel, n), out_shape=jax.ShapeDtypeStru...]
    all_gather x4 -> x0, blocking collectives: 65 us -> none  [the longest x1 18.8 us: on_device(): lax.all_gather(sw_value_weight, 'sp', axis=0, tiled=True)]
    all_gather x4 -> x0, waiting for transfers between devices: 60.3 us -> none  [the longest x1 26.9 us: on_device(): lax.all_gather(sw_query_weight, 'sp', axis=0, tiled=True)]
    psum x1 -> x0, waiting for transfers between devices: 38.9 us -> none  [on_device(): return lax.psum(partial_value.astype(jnp.bfloat16), 'tp')]
    dot_general x14 -> x0, matrix products: 14 us -> none  [the longest x6 8.74 us: on_device(): jnp.dot(normed, piece, preferred_element_type=jnp.float32)]
    ppermute x2 -> x0, starting transfers between devices: 4.53 us -> none  [shifted(): lax.ppermute(value, axis, [(source, source + steps) for source in range(f...]
    reduce_sum x5 -> x0, other arithmetic: 3.01 us -> none  [the longest x2 1.58 us: rms_norm(): jnp.mean(values * values, axis=-1, keepdims=True) + 1e-06]
  transfers between devices with their start and end apart: 7 -> 0, of which waited for: 4 -> 0; matrix products, arithmetic and copies ran while one was open for 9% -> 0% of each run, Pallas kernels for 0% -> 0%
where the time goes in v1:
time: 83.4 us; the launch traced here: 81.9 us
  Pallas kernels  73 us (88%)
  local copies, waits for them, and re-layouts  7.43 us (9%)
  other arithmetic  1.31 us (2%)
    pallas_call x1, Pallas kernels, transposed(): pl.pallas_call(functools.partial(kernel, n), out_shape=jax.ShapeDtypeStru...  73 us
    unnamed x19, local copies, waits for them, and re-layouts  2.36 us

profile of v1, /device:TPU:1, one launch (start us, length us, event | category | flops | bytes accessed | tf_op | source)
XLA Modules:
  0.0 81.9 jit_solution(5321771167136342406)
XLA Ops:
  0.0 1.3 %fusion.4 = (bf16[512,64]{1,0:T(8,128)(2,1)S(1)}, bf16[512,64]{1,0:T(8,128)(2,1)S(1)}, bf16[512,64]{1,0:T(8,128)(2,1)S(1)}, bf16[512,64]{1,0:T(8,128)(2,1)S(1)}) fusion(bf16[512,128]{1,0:T(8,128)(2,1)} %param.24, bf16[512,128]{1,0:T(8,128)(2,1)} %param.23), kind=kLoop, calls=%fused_computation.6 | loop fusion | bytes 524288 | tf_op jit(solution)/shard_map/slice | solution.py:599
  1.3 1.1 %fusion = (bf16[512,128]{1,0:T(8,128)(2,1)S(1)}, bf16[512,128]{1,0:T(8,128)(2,1)S(1)}, bf16[512,128]{1,0:T(8,128)(2,1)S(1)}, bf16[512,128]{1,0:T(8,128)(2,1)S(1)}) fusion(bf16[512,256]{1,0:T(8,128)(2,1)} %param.22, bf16[512,256]{1,0:T(8,128)(2,1)} %param.21), kind=kLoop, calls=%fused_computation.2 | loop fusion | bytes 1048576 | tf_op jit(solution)/shard_map/slice | solution.py:597
  2.5 0.1 fusion.2
  2.6 0.3 concatenate.10
  2.9 0.3 concatenate.11
  3.3 0.0 copy-start.3
  3.3 0.0 copy-start.4
  3.3 0.0 copy-start.5
  3.3 0.0 copy-start.6
  3.3 0.0 copy-start.7
  3.3 0.0 copy-start.8
  3.3 1.2 %pad_maximum_fusion.w_ref = bf16[2,2,2,128,640]{4,3,2,1,0:T(8,128)(2,1)} fusion(bf16[1,2,2,128,640]{4,3,2,1,0:T(8,128)(2,1)S(1)} %bitcast.9, bf16[1,2,2,128,640]{4,3,2,1,0:T(8,128)(2,1)S(1)} %bitcast.8), kind=kLoop, calls=%fused_computation | loop fusion | flops 655360 | bytes 2621440 | tf_op jit(solution)/shard_map/stack | solution.py:606
  4.6 0.1 copy.18
  4.7 0.1 pad.2.clone
  4.8 0.1 reshape.28
  4.8 0.1 maximum_maximum_fusion
  4.9 0.7 broadcast_in_dim.2.scalars_ref
  5.6 0.1 stack_tile.12
  5.7 0.1 stack_tile.13
  5.8 0.1 stack_tile.14
  5.9 0.1 stack_tile.15
  5.9 0.6 stack.22.gains_ref
  6.6 73.0 %shard_map.163 = bf16[2,128,2048]{2,1,0:T(8,128)(2,1)} custom-call(bf16[2,2,64,2048]{3,2,1,0:T(8,128)(2,1)} %bitcast.10, bf16[2,2,2,128,640]{4,3,2,1,0:T(8,128)(2,1)} %pad_maximum_fusion.w_ref, f32[1,2048]{1,0:T(1,128)} %bitcast.11, f32[8,128]{1,0:T(8,128)} %stack.22.gains_ref, f32[2,8,128]{2,1,0:T(8,128)} %broadcast_in_dim.2.scalars_ref, ...), custom_call_target="tpu_custom_call" | custom-call | tf_op jit(solution)/shard_map/pallas_call | solution.py:626
  79.6 2.3 %copy.20 = bf16[256,2048]{1,0:T(8,128)(2,1)} copy(bf16[256,2048]{1,0:T(8,128)(2,1)} %bitcast.7) | data formatting | bytes 2097152
  (17 shorter events, 0.0 us)
Async XLA Ops:
  0.0 2.4 %copy-start.1 = (bf16[512,256]{1,0:T(8,128)(2,1)S(1)}, bf16[512,256]{1,0:T(8,128)(2,1)}, u32[]{:S(2)}) copy-start(bf16[512,256]{1,0:T(8,128)(2,1)} %param.19) | copy-start | bytes 786436
  0.0 2.5 %copy-start = (bf16[512,256]{1,0:T(8,128)(2,1)S(1)}, bf16[512,256]{1,0:T(8,128)(2,1)}, u32[]{:S(2)}) copy-start(bf16[512,256]{1,0:T(8,128)(2,1)} %param.20) | copy-start | bytes 786436
  3.3 1.3 %copy-start.3 = (f32[2]{0:T(128)S(1)}, f32[2]{0:T(128)}, u32[]{:S(2)}) copy-start(f32[2]{0:T(128)} %param.29) | copy-start | bytes 28
  3.3 1.5 %copy-start.4 = (f32[4]{0:T(128)S(1)}, f32[4]{0:T(128)}, u32[]{:S(2)}) copy-start(f32[4]{0:T(128)} %param.31) | copy-start | bytes 52
  3.3 2.3 %copy-start.5 = (f32[64]{0:T(128)S(1)}, f32[64]{0:T(128)}, u32[]{:S(2)}) copy-start(f32[64]{0:T(128)} %param.25) | copy-start | bytes 772
  3.3 2.4 %copy-start.6 = (f32[64]{0:T(128)S(1)}, f32[64]{0:T(128)}, u32[]{:S(2)}) copy-start(f32[64]{0:T(128)} %param.26) | copy-start | bytes 772
  3.3 2.5 %copy-start.7 = (f32[64]{0:T(128)S(1)}, f32[64]{0:T(128)}, u32[]{:S(2)}) copy-start(f32[64]{0:T(128)} %param.27) | copy-start | bytes 772
  3.3 2.5 %copy-start.8 = (f32[64]{0:T(128)S(1)}, f32[64]{0:T(128)}, u32[]{:S(2)}) copy-start(f32[64]{0:T(128)} %param.28) | copy-start | bytes 772
  3.3 2.6 %copy-start.2 = (f32[128]{0:T(128)S(1)}, f32[128]{0:T(128)}, u32[]{:S(2)}) copy-start(f32[128]{0:T(128)} %param.30) | copy-start | bytes 1540

commit v2 on v1

--- a/solution.py
+++ b/solution.py
@@ -207,13 +207,27 @@
 def kernel(
     n,
     x_ref,
-    w_ref,
+    da_q_ref,
+    da_k_ref,
+    da_v_ref,
+    sw_q_ref,
+    sw_k_ref,
+    sw_v_ref,
     norm_gain_ref,
-    gains_ref,
-    scalars_ref,
+    da_q_gain_ref,
+    da_k_gain_ref,
+    sw_q_gain_ref,
+    sw_k_gain_ref,
+    head_gain_ref,
+    mix_ref,
+    sink_ref,
+    da_out_hbm,
+    sw_out_hbm,
+    out_ref,
     da_out_ref,
     sw_out_ref,
-    out_ref,
+    small,
+    gains_ref,
     xg,
     wb,
     normed,
@@ -285,6 +299,27 @@
     for k in range(1, n):
         for cc in range(CORES):
             greet(at(lax.rem(z + k, n), cc))
+
+    own_x = pltpu.make_async_copy(x_ref.at[c], xg.at[z], local_sem.at[1])
+    own_x.start()
+    out_loads = [
+        pltpu.make_async_copy(da_out_hbm, da_out_ref, local_sem.at[4]),
+        pltpu.make_async_copy(sw_out_hbm, sw_out_ref, local_sem.at[5]),
+    ]
+    for load in out_loads:
+        load.start()
+
+    wide = 2 * HD
+    for par in range(CORES):
+        cols = slice(par * HD, (par + 1) * HD)
+        small[par] = jnp.concatenate([sw_k_ref[..., cols], sw_v_ref[..., cols]], axis=-1)
+        scal[c, par, 0:1, :] = jnp.broadcast_to(mix_ref[:, par : par + 1], (1, wide))
+        for g in range(2):
+            sink = sink_ref[:, 2 * par + g : 2 * par + g + 1]
+            scal[c, par, 1 + g : 2 + g, :] = jnp.broadcast_to(sink, (1, wide))
+    for i, ref in enumerate((da_q_gain_ref, da_k_gain_ref, sw_q_gain_ref, sw_k_gain_ref)):
+        gains_ref[i : i + 1, :] = jnp.concatenate([ref[...], ref[...]], axis=-1)
+    gains_ref[4:5, :] = head_gain_ref[...]
     pl.semaphore_wait(barrier, 3 + (n - 1) * CORES)
 
     pending = []
@@ -296,13 +331,15 @@
             pl.when(when)(copy.start)
         pending.append((copy, when))
 
-    def hop(d, k):
+    pieces = xg.shape[2]
+
+    def hop(d, k, p):
         source = z - k if d == 0 else z + k
         source = jnp.clip(source, 0, n - 1)
         target = jnp.clip(z + 1 if d == 0 else z - 1, 0, n - 1)
-        src = x_ref.at[c, x] if k == 0 else xg.at[source, x]
+        src = x_ref.at[c, x, p] if k == 0 else xg.at[source, x, p]
         return remote(
-            src, xg.at[source, x], x_send.at[d, k], x_recv.at[d, k], {"sp": target}
+            src, xg.at[source, x, p], x_send.at[d, k, p], x_recv.at[d, k, p], {"sp": target}
         )
 
     def can_hop(d, k):
@@ -311,39 +348,55 @@
     def has(d, k):
         return z - k >= 0 if d == 0 else z + k < n
 
-    go(hop(0, 0), can_hop(0, 0))
-    go(hop(1, 0), can_hop(1, 0))
-
-    for par in range(CORES):
-        zt = CORES * c + par
-        for cd in range(CORES):
-            go(
-                remote(
-                    w_ref.at[par, y, cd],
-                    wb.at[z, y, cd],
-                    w_send.at[par, cd],
-                    w_recv.at[z],
-                    at(zt, cd),
-                ),
-                zt != z,
-            )
+    def from_there(d, k):
+        return jnp.clip(z - k if d == 0 else z + k, 0, n - 1)
+
+    for p in range(pieces):
+        for d in range(2):
+            go(hop(d, 0, p), can_hop(d, 0))
+
     owner = c == z // CORES
-    own = remote(w_ref.at[z % CORES], wb.at[z], own_send, own_recv, peer)
-    go(own, owner)
-    own_local = pltpu.make_async_copy(w_ref.at[z % CORES], wb.at[z], local_sem.at[0])
-    pl.when(owner)(own_local.start)
-    own_x = pltpu.make_async_copy(x_ref.at[c], xg.at[z], local_sem.at[1])
-    own_x.start()
-    sc_local = pltpu.make_async_copy(scalars_ref, scal.at[c], local_sem.at[2])
-    sc_local.start()
-    sc = remote(scalars_ref, scal.at[c], sc_send, sc_recv, peer)
+
+    def columns_of(par, yy, cc):
+        found = [
+            ref.at[yy, cc, :, pl.ds(pl.multiple_of(par * wide, wide), wide)]
+            for ref in (da_q_ref, da_k_ref, da_v_ref, sw_q_ref)
+        ]
+        return found + [small.at[par, yy, cc]]
+
+    def own_copies(kind):
+        copies = []
+        for yy in range(2):
+            for cc in range(CORES):
+                for j, src in enumerate(columns_of(z % CORES, yy, cc)):
+                    dst = wb.at[z, yy, cc, :, pl.ds(j * wide, wide)]
+                    if kind == 0:
+                        copies.append(pltpu.make_async_copy(src, dst, local_sem.at[0]))
+                    else:
+                        copies.append(remote(src, dst, own_send, own_recv, peer))
+        return copies
+
+    own = remote(wb.at[z], wb.at[z], own_send, own_recv, peer)
+    own_local = pltpu.make_async_copy(wb.at[z], wb.at[z], local_sem.at[0])
+
+    @pl.when(owner)
+    def _():
+        for copy in own_copies(0) + own_copies(1):
+            copy.start()
+
+    pending.append((own, owner))
+    sc = remote(scal.at[c], scal.at[c], sc_send, sc_recv, peer)
     go(sc)
 
-    def cross(zs):
-        return remote(xg.at[zs, x], xg.at[zs, x], xf_send.at[zs], xf_recv.at[zs], across)
-
-    def weight_direct(zs):
-        return remote(wb.at[zs, y, c], wb.at[zs, y, c], w_send.at[0, 0], w_recv.at[zs], peer)
+    def cross(zs, p):
+        return remote(
+            xg.at[zs, x, p], xg.at[zs, x, p], xf_send.at[zs, p], xf_recv.at[zs, p], across
+        )
+
+    def weight_direct(zs, par=0, cd=0):
+        return remote(
+            wb.at[zs, y, c], wb.at[zs, y, c], w_send.at[par, cd], w_recv.at[zs], peer
+        )
 
     def weight_beside(zs):
         return remote(wb.at[zs, y, c], wb.at[zs, y, c], wy_send.at[zs], wy_recv.at[zs], beside)
@@ -354,43 +407,98 @@
             wb.at[zs, yy, c], wb.at[zs, yy, c], wc_send.at[which, zs], wc_recv.at[which, zs], peer
         )
 
+    def pass_on(k):
+        for p in range(pieces):
+            for d in range(2):
+                zs = from_there(d, k)
+
+                def arrived(zs=zs, d=d, p=p):
+                    remote(
+                        xg.at[zs, x, p],
+                        xg.at[zs, x, p],
+                        x_send.at[d, k - 1, p],
+                        x_recv.at[d, k - 1, p],
+                        across,
+                    ).wait_recv()
+
+                pl.when(has(d, k))(arrived)
+                if k < n - 1:
+                    go(hop(d, k, p), can_hop(d, k))
+                go(cross(zs, p), has(d, k))
+
+    def send_weights():
+        for par in range(CORES):
+            zt = CORES * c + par
+            for cd in range(CORES):
+
+                @pl.when(zt != z)
+                def _(par=par, cd=cd, zt=zt):
+                    for j, src in enumerate(columns_of(par, y, cd)):
+                        remote(
+                            src,
+                            wb.at[z, y, cd, :, pl.ds(j * wide, wide)],
+                            w_send.at[par, cd],
+                            w_recv.at[z],
+                            at(zt, cd),
+                        ).start()
+
+                pending.append((weight_direct(z, par, cd), zt != z))
+
+    def pass_weights(k):
+        for d in range(2):
+            zs = from_there(d, k)
+            pl.when(has(d, k))(lambda zs=zs: weight_direct(zs).wait_recv())
+            go(weight_beside(zs), has(d, k))
+            go(weight_core(zs, 0), has(d, k))
+
+    part = xg.shape[2] * xg.shape[3]
+    tile = 2 * part
+
+    def norm_of(i):
+        for h in range(2):
+            values = xg[i, h].reshape(part, xg.shape[4]).astype(F32)
+            values = rms_norm(values, norm_gain_ref[...])
+            normed[i, h * part : (h + 1) * part, :] = values.astype(BF16)
+
+    pass_on(1)
+    send_weights()
+    pass_on(2)
+    pass_weights(1)
+    pass_weights(2)
+    own_x.wait()
+    norm_of(z)
+    pass_on(3)
+    pass_weights(3)
+    others = [lax.rem(z + k, n) for k in range(1, n)]
     for k in range(1, n):
         for d in range(2):
-            there = has(d, k)
-            zs = jnp.clip(z - k if d == 0 else z + k, 0, n - 1)
-
-            def arrived(zs=zs, d=d, k=k):
+            zs = from_there(d, k)
+
+            @pl.when(has(d, k))
+            def _(zs=zs):
                 remote(
-                    xg.at[zs, x], xg.at[zs, x], x_send.at[d, k - 1], x_recv.at[d, k - 1], across
+                    wb.at[zs, 1 - y, c],
+                    wb.at[zs, 1 - y, c],
+                    wy_send.at[zs],
+                    wy_recv.at[zs],
+                    beside,
                 ).wait_recv()
 
-            pl.when(there)(arrived)
-            if k < n - 1:
-                go(hop(d, k), can_hop(d, k))
-            go(cross(zs), there)
+            go(weight_core(zs, 1), has(d, k))
+    for k in range(1, n):
         for d in range(2):
-            there = has(d, k)
-            zs = jnp.clip(z - k if d == 0 else z + k, 0, n - 1)
-            pl.when(there)(lambda zs=zs: weight_direct(zs).wait_recv())
-            go(weight_beside(zs), there)
-            go(weight_core(zs, 0), there)
-    others = [lax.rem(z + k, n) for k in range(1, n)]
-    for zs in others:
-        remote(wb.at[zs, 1 - y, c], wb.at[zs, 1 - y, c], wy_send.at[zs], wy_recv.at[zs], beside).wait_recv()
-        go(weight_core(zs, 1))
-    for zs in others:
-        remote(
-            xg.at[zs, 1 - x], xg.at[zs, 1 - x], xf_send.at[zs], xf_recv.at[zs], across
-        ).wait_recv()
-    own_x.wait()
-
-    part = xg.shape[2]
-    tile = 2 * part
-    for i in range(n):
-        for h in range(2):
-            values = xg[i, h].astype(F32)
-            values = rms_norm(values, norm_gain_ref[...])
-            normed[i, h * part : (h + 1) * part, :] = values.astype(BF16)
+
+            @pl.when(has(d, k))
+            def _(zs=from_there(d, k)):
+                for p in range(pieces):
+                    remote(
+                        xg.at[zs, 1 - x, p],
+                        xg.at[zs, 1 - x, p],
+                        xf_send.at[zs, p],
+                        xf_recv.at[zs, p],
+                        across,
+                    ).wait_recv()
+                norm_of(zs)
 
     pl.when(owner)(own_local.wait)
     pl.when(jnp.logical_not(owner))(own.wait_recv)
@@ -406,7 +514,6 @@
             ).wait_recv()
 
     depth = wb.shape[1] * wb.shape[2] * wb.shape[3]
-    wide = 2 * HD
     width = wb.shape[4]
     for i in range(n):
         acc = dot(normed[i, :, 0:depth], wb[0].reshape(depth, width))
@@ -428,39 +535,26 @@
 
     swap = remote(kv.at[c], kv.at[c], kv_send, kv_recv, peer)
     go(swap)
-    sc_local.wait()
     remote(scal.at[1 - c], scal.at[1 - c], sc_send, sc_recv, peer).wait_recv()
     remote(kv.at[1 - c], kv.at[1 - c], kv_send, kv_recv, peer).wait_recv()
 
     mine = scal[z // CORES, z % CORES]
     mix = mine[0:1, :]
+    def send_rows(i, j):
+        cols = pl.ds(j * wide, wide)
+        away = (z != i) | jnp.logical_not(owner)
+        go(
+            remote(
+                rows_out.at[i, :, cols],
+                rows_in.at[z % CORES, c, :, cols],
+                r_send.at[i, j],
+                r_recv.at[z % CORES, c, j],
+                at(i, z // CORES),
+            ),
+            away,
+        )
+
     for i in range(n):
-        q_place = (2 * i + c) * tile + lax.broadcasted_iota(jnp.int32, (tile, 1), 0)
-        count = (i + 1) * tile
-        column = lax.broadcasted_iota(jnp.int32, (1, count), 1)
-        maps = []
-        for m in range(2):
-            q = query[i, :, m * HD : (m + 1) * HD]
-            scores = []
-            for h in range(2):
-                keys = kv[h, 0 : i + 1, :, m * HD : (m + 1) * HD].reshape(count, HD)
-                place = (column // tile) * (2 * tile) + h * tile + column % tile
-                scores.append(jnp.where(place <= q_place, dot_t(q, keys), -jnp.inf))
-            top = jnp.maximum(
-                jnp.max(scores[0], axis=-1, keepdims=True),
-                jnp.max(scores[1], axis=-1, keepdims=True),
-            )
-            total = 0.0
-            summed = 0.0
-            for h in range(2):
-                weights = jnp.exp(scores[h] - top)
-                total += jnp.sum(weights, axis=-1, keepdims=True)
-                values = kv[h, 0 : i + 1, :, wide : 2 * wide].reshape(count, wide)
-                summed += dot(weights.astype(BF16), values)
-            maps.append(summed / total)
-        blend = maps[0] - mix * maps[1]
-        rows_out[i, :, 0:wide] = rms_norm(blend, gains_ref[4:5, :]).astype(BF16)
-
         before = jnp.maximum(i - 1 + c, 0)
         q_row = lax.broadcasted_iota(jnp.int32, (tile, tile), 0)
         k_row = lax.broadcasted_iota(jnp.int32, (tile, tile), 1)
@@ -490,17 +584,37 @@
             results.append(summed / total)
         rows_out[i, :, wide : 2 * wide] = jnp.concatenate(results, axis=-1).astype(BF16)
 
-        away = (z != i) | jnp.logical_not(owner)
-        go(
-            remote(
-                rows_out.at[i],
-                rows_in.at[z % CORES, c],
-                r_send.at[i],
-                r_recv.at[z % CORES, c],
-                at(i, z // CORES),
-            ),
-            away,
-        )
+        send_rows(i, 1)
+
+    for i in range(n):
+        q_place = (2 * i + c) * tile + lax.broadcasted_iota(jnp.int32, (tile, 1), 0)
+        count = (i + 1) * tile
+        column = lax.broadcasted_iota(jnp.int32, (1, count), 1)
+        maps = []
+        for m in range(2):
+            q = query[i, :, m * HD : (m + 1) * HD]
+            scores = []
+            for h in range(2):
+                keys = kv[h, 0 : i + 1, :, m * HD : (m + 1) * HD].reshape(count, HD)
+                place = (column // tile) * (2 * tile) + h * tile + column % tile
+                scores.append(jnp.where(place <= q_place, dot_t(q, keys), -jnp.inf))
+            top = jnp.maximum(
+                jnp.max(scores[0], axis=-1, keepdims=True),
+                jnp.max(scores[1], axis=-1, keepdims=True),
+            )
+            total = 0.0
+            summed = 0.0
+            for h in range(2):
+                weights = jnp.exp(scores[h] - top)
+                total += jnp.sum(weights, axis=-1, keepdims=True)
+                values = kv[h, 0 : i + 1, :, wide : 2 * wide].reshape(count, wide)
+                summed += dot(weights.astype(BF16), values)
+            maps.append(summed / total)
+        blend = maps[0] - mix * maps[1]
+        rows_out[i, :, 0:wide] = rms_norm(blend, gains_ref[4:5, :]).astype(BF16)
+
+        send_rows(i, 0)
+
     keep_rows = pltpu.make_async_copy(rows_out.at[z], rows_in.at[z % CORES, c], local_sem.at[3])
     pl.when(owner)(keep_rows.start)
     pl.when(owner)(keep_rows.wait)
@@ -509,9 +623,15 @@
         for par in range(CORES):
 
             def wait(par=par):
-                remote(
-                    rows_in.at[par, cc], rows_in.at[par, cc], r_send.at[0], r_recv.at[par, cc], peer
-                ).wait_recv()
+                for j in range(2):
+                    cols = pl.ds(j * wide, wide)
+                    remote(
+                        rows_in.at[par, cc, :, cols],
+                        rows_in.at[par, cc, :, cols],
+                        r_send.at[0, j],
+                        r_recv.at[par, cc, j],
+                        peer,
+                    ).wait_recv()
 
             pl.when((CORES * c + par != z) | (cc != c))(wait)
 
@@ -526,6 +646,8 @@
             acc += dot(rows[:, wide : 2 * wide], sw_out_ref[par * wide : (par + 1) * wide, cols])
         return acc.astype(BF16)
 
+    for load in out_loads:
+        load.wait()
     await_rows(1 - c)
     for q in range(4):
         part_out[:, q * columns : (q + 1) * columns] = project(1 - c, q)
@@ -584,52 +706,32 @@
     rows, d = inputs.shape
     depth = da_query_weight.shape[0]
     wide = 2 * HD
-    packed = []
-    for par in range(CORES):
-        big = slice(par * wide, (par + 1) * wide)
-        small = slice(par * HD, (par + 1) * HD)
-        packed.append(
-            jnp.concatenate(
-                [
-                    da_query_weight[:, big],
-                    da_key_weight[:, big],
-                    da_value_weight[:, big],
-                    sw_query_weight[:, big],
-                    sw_key_weight[:, small],
-                    sw_value_weight[:, small],
-                ],
-                axis=1,
-            )
-        )
-    width = packed[0].shape[1]
+    width = 5 * wide
     piece = depth // 4
-    weights = jnp.stack(packed).reshape(CORES, 2, CORES, piece, width)
-    gains = jnp.stack(
-        [
-            jnp.tile(da_query_gain, 2),
-            jnp.tile(da_key_gain, 2),
-            jnp.tile(sw_query_gain, 2),
-            jnp.tile(sw_key_gain, 2),
-            head_gain,
-            head_gain,
-            head_gain,
-            head_gain,
-        ]
-    )
-    sinks = sink_logit.reshape(CORES, 2)
-    scalars = jnp.concatenate([mix_lambda.reshape(CORES, 1), sinks, jnp.zeros((CORES, 5), F32)], axis=1)
-    scalars = jnp.broadcast_to(scalars[:, :, None], (CORES, 8, wide))
+
+    def cut(weight):
+        return weight.reshape(2, CORES, piece, weight.shape[1])
+
+    def line(vector):
+        return vector.reshape(1, -1)
+
+    pieces = 4
     part = rows // 4
     tile = rows // 2
     DMA = pltpu.SemaphoreType.DMA
     vmem = pl.BlockSpec(memory_space=pltpu.VMEM)
+    hbm = pl.BlockSpec(memory_space=pl.ANY)
     out = pl.pallas_call(
         functools.partial(kernel, n),
         out_shape=jax.ShapeDtypeStruct((2, tile, d), BF16),
-        in_specs=[vmem] * 7,
+        in_specs=[hbm] * 5 + [vmem] * 10 + [hbm] * 2,
         out_specs=vmem,
         scratch_shapes=[
-            pltpu.VMEM((n, 2, part, d), BF16),
+            pltpu.VMEM(da_out_weight.shape, BF16),
+            pltpu.VMEM(sw_out_weight.shape, BF16),
+            pltpu.VMEM((CORES, 2, CORES, piece, wide), BF16),
+            pltpu.VMEM((8, wide), F32),
+            pltpu.VMEM((n, 2, pieces, part // pieces, d), BF16),
             pltpu.VMEM((n, 2, CORES, piece, width), BF16),
             pltpu.VMEM((n, tile, d), BF16),
             pltpu.VMEM((n, tile, 2 * wide), BF16),
@@ -641,11 +743,11 @@
             pltpu.VMEM((tile, d), BF16),
             pltpu.VMEM((tile, d), BF16),
             pltpu.VMEM((tile, d), BF16),
-            DMA((4,)),
-            DMA((2, n)),
-            DMA((2, n)),
-            DMA((n,)),
-            DMA((n,)),
+            DMA((6,)),
+            DMA((2, n, pieces)),
+            DMA((2, n, pieces)),
+            DMA((n, pieces)),
+            DMA((n, pieces)),
             DMA((CORES, CORES)),
             DMA((n,)),
             DMA((n,)),
@@ -658,8 +760,8 @@
             DMA,
             DMA,
             DMA,
-            DMA((n,)),
-            DMA((CORES, CORES)),
+            DMA((n, 2)),
+            DMA((CORES, CORES, 2)),
             DMA((4,)),
             DMA((4,)),
             DMA((4,)),
@@ -671,11 +773,21 @@
             collective_id=0, has_side_effects=True, vmem_limit_bytes=60 * 1024 * 1024
         ),
     )(
-        inputs.reshape(CORES, 2, part, d),
-        weights,
-        norm_gain.reshape(1, d),
-        gains,
-        scalars,
+        inputs.reshape(CORES, 2, pieces, part // pieces, d),
+        cut(da_query_weight),
+        cut(da_key_weight),
+        cut(da_value_weight),
+        cut(sw_query_weight),
+        cut(sw_key_weight),
+        cut(sw_value_weight),
+        line(norm_gain),
+        line(da_query_gain),
+        line(da_key_gain),
+        line(sw_query_gain),
+        line(sw_key_gain),
+        line(head_gain),
+        line(mix_lambda),
+        line(sink_logit),
         da_out_weight,
         sw_out_weight,
     )

time: 83.4 us -> 78.1 us (0.936)
  local copies, waits for them, and re-layouts: 7.43 us -> 2.3 us
  Pallas kernels: 73 us -> 74.5 us
  other arithmetic: 1.31 us -> 0 us
    slice x3 -> x0, local copies, waits for them, and re-layouts: 2.51 us -> none  [the longest x1 1.29 us: transposed(): sw_value_weight[:, small]]
    pallas_call x1, Pallas kernels: 73 us -> 74.5 us  [transposed(): pl.pallas_call(functools.partial(kernel, n), out_shape=jax.ShapeDtypeStru...]
    another operation x1 -> x0, other arithmetic: 1.23 us -> none  [transposed(): weights = jnp.stack(packed).reshape(CORES, 2, CORES, piece, width)]
    another operation x10 -> x0, local copies, waits for them, and re-layouts: 0.95 us -> none  [the longest x5 0.94 us: transposed(): jnp.stack([jnp.tile(da_query_gain, 2), jnp.tile(da_key_gain, 2), jnp.tile...]
    unnamed x19 -> x1, local copies, waits for them, and re-layouts: 2.36 us -> 2.3 us
where the time goes in v2:
time: 78.1 us; the launch traced here: 76.8 us
  Pallas kernels  74.5 us (95%)
  local copies, waits for them, and re-layouts  2.3 us (3%)
    pallas_call x1, Pallas kernels, transposed(): pl.pallas_call(functools.partial(kernel, n), out_shape=jax.ShapeDtypeStru...  74.5 us
    unnamed x1, local copies, waits for them, and re-layouts  2.3 us

profile of v2, /device:TPU:1, one launch (start us, length us, event | category | flops | bytes accessed | tf_op | source)
XLA Modules:
  0.0 76.8 jit_solution(14977617624428383331)
XLA Ops:
  0.0 74.5 %shard_map.163 = bf16[2,128,2048]{2,1,0:T(8,128)(2,1)} custom-call(bf16[2,2,4,16,2048]{4,3,2,1,0:T(8,128)(2,1)} %bitcast.17, bf16[2,2,128,256]{3,2,1,0:T(8,128)(2,1)} %bitcast.18, bf16[2,2,128,256]{3,2,1,0:T(8,128)(2,1)} %bitcast.19, bf16[2,2,128,256]{3,2,1,0:T(8,128)(2,1)} %bitcast.20, bf16[2,2,128,256]{3,2,1,0:T(8,128)(2,1)} %bitcast.21, ...), custom_call_target="tpu_custom_call" | custom-call | tf_op jit(solution)/shard_map/pallas_call | solution.py:724
  74.5 2.3 %copy.19 = bf16[256,2048]{1,0:T(8,128)(2,1)} copy(bf16[256,2048]{1,0:T(8,128)(2,1)} %bitcast.16) | data formatting | bytes 2097152

commit v3 on v2

--- a/solution.py
+++ b/solution.py
@@ -226,7 +226,7 @@
     out_ref,
     da_out_ref,
     sw_out_ref,
-    small,
+    wp,
     gains_ref,
     xg,
     wb,
@@ -310,9 +310,22 @@
         load.start()
 
     wide = 2 * HD
+    packs = []
+    for par in range(CORES):
+        for j, ref in enumerate((da_q_ref, da_k_ref, da_v_ref, sw_q_ref)):
+            packs.append(
+                pltpu.make_async_copy(
+                    ref.at[:, :, :, :, pl.ds(par * wide, wide)],
+                    wp.at[par, :, :, :, :, pl.ds(j * wide, wide)],
+                    local_sem.at[6 + par * 4 + j],
+                )
+            )
+    for pack in packs:
+        pack.start()
+
     for par in range(CORES):
         cols = slice(par * HD, (par + 1) * HD)
-        small[par] = jnp.concatenate([sw_k_ref[..., cols], sw_v_ref[..., cols]], axis=-1)
+        wp[par, :, :, :, :, 4 * wide : 5 * wide] = jnp.concatenate([sw_k_ref[..., cols], sw_v_ref[..., cols]], axis=-1)
         scal[c, par, 0:1, :] = jnp.broadcast_to(mix_ref[:, par : par + 1], (1, wide))
         for g in range(2):
             sink = sink_ref[:, 2 * par + g : 2 * par + g + 1]
@@ -337,7 +350,7 @@
         source = z - k if d == 0 else z + k
         source = jnp.clip(source, 0, n - 1)
         target = jnp.clip(z + 1 if d == 0 else z - 1, 0, n - 1)
-        src = x_ref.at[c, x, p] if k == 0 else xg.at[source, x, p]
+        src = xg.at[source, x, p]
         return remote(
             src, xg.at[source, x, p], x_send.at[d, k, p], x_recv.at[d, k, p], {"sp": target}
         )
@@ -351,40 +364,18 @@
     def from_there(d, k):
         return jnp.clip(z - k if d == 0 else z + k, 0, n - 1)
 
+    own_x.wait()
     for p in range(pieces):
         for d in range(2):
             go(hop(d, 0, p), can_hop(d, 0))
 
     owner = c == z // CORES
 
-    def columns_of(par, yy, cc):
-        found = [
-            ref.at[yy, cc, :, pl.ds(pl.multiple_of(par * wide, wide), wide)]
-            for ref in (da_q_ref, da_k_ref, da_v_ref, sw_q_ref)
-        ]
-        return found + [small.at[par, yy, cc]]
-
-    def own_copies(kind):
-        copies = []
-        for yy in range(2):
-            for cc in range(CORES):
-                for j, src in enumerate(columns_of(z % CORES, yy, cc)):
-                    dst = wb.at[z, yy, cc, :, pl.ds(j * wide, wide)]
-                    if kind == 0:
-                        copies.append(pltpu.make_async_copy(src, dst, local_sem.at[0]))
-                    else:
-                        copies.append(remote(src, dst, own_send, own_recv, peer))
-        return copies
-
-    own = remote(wb.at[z], wb.at[z], own_send, own_recv, peer)
-    own_local = pltpu.make_async_copy(wb.at[z], wb.at[z], local_sem.at[0])
-
-    @pl.when(owner)
-    def _():
-        for copy in own_copies(0) + own_copies(1):
-            copy.start()
-
-    pending.append((own, owner))
+    for pack in packs:
+        pack.wait()
+    own = remote(wp.at[z % CORES], wb.at[z], own_send, own_recv, peer)
+    own_local = pltpu.make_async_copy(wp.at[z % CORES], wb.at[z], local_sem.at[0])
+
     sc = remote(scal.at[c], scal.at[c], sc_send, sc_recv, peer)
     go(sc)
 
@@ -393,63 +384,65 @@
             xg.at[zs, x, p], xg.at[zs, x, p], xf_send.at[zs, p], xf_recv.at[zs, p], across
         )
 
-    def weight_direct(zs, par=0, cd=0):
+    def weight_direct(zs, s):
         return remote(
-            wb.at[zs, y, c], wb.at[zs, y, c], w_send.at[par, cd], w_recv.at[zs], peer
+            wb.at[zs, y, c, s], wb.at[zs, y, c, s], w_send.at[0, 0, s], w_recv.at[zs, s], peer
         )
 
-    def weight_beside(zs):
-        return remote(wb.at[zs, y, c], wb.at[zs, y, c], wy_send.at[zs], wy_recv.at[zs], beside)
-
-    def weight_core(zs, which):
-        yy = y if which == 0 else 1 - y
+    def weight_beside(zs, yy, s):
         return remote(
-            wb.at[zs, yy, c], wb.at[zs, yy, c], wc_send.at[which, zs], wc_recv.at[which, zs], peer
+            wb.at[zs, yy, c, s], wb.at[zs, yy, c, s], wy_send.at[zs, s], wy_recv.at[zs, s], beside
         )
 
-    def pass_on(k):
-        for p in range(pieces):
-            for d in range(2):
-                zs = from_there(d, k)
-
-                def arrived(zs=zs, d=d, p=p):
-                    remote(
-                        xg.at[zs, x, p],
-                        xg.at[zs, x, p],
-                        x_send.at[d, k - 1, p],
-                        x_recv.at[d, k - 1, p],
-                        across,
-                    ).wait_recv()
-
-                pl.when(has(d, k))(arrived)
-                if k < n - 1:
-                    go(hop(d, k, p), can_hop(d, k))
-                go(cross(zs, p), has(d, k))
-
-    def send_weights():
+    def weight_core(zs, which, cc, s):
+        ref = wb.at[zs, y if which == 0 else 1 - y, cc, s]
+        return remote(ref, ref, wc_send.at[which, zs, s], wc_recv.at[which, zs, s], peer)
+
+    def pass_on(k, p):
+        for d in range(2):
+            zs = from_there(d, k)
+
+            def arrived(zs=zs, d=d):
+                remote(
+                    xg.at[zs, x, p],
+                    xg.at[zs, x, p],
+                    x_send.at[d, k - 1, p],
+                    x_recv.at[d, k - 1, p],
+                    across,
+                ).wait_recv()
+
+            pl.when(has(d, k))(arrived)
+            if k < n - 1:
+                go(hop(d, k, p), can_hop(d, k))
+            go(cross(zs, p), has(d, k))
+
+    def send_weights(s):
         for par in range(CORES):
             zt = CORES * c + par
             for cd in range(CORES):
-
-                @pl.when(zt != z)
-                def _(par=par, cd=cd, zt=zt):
-                    for j, src in enumerate(columns_of(par, y, cd)):
-                        remote(
-                            src,
-                            wb.at[z, y, cd, :, pl.ds(j * wide, wide)],
-                            w_send.at[par, cd],
-                            w_recv.at[z],
-                            at(zt, cd),
-                        ).start()
-
-                pending.append((weight_direct(z, par, cd), zt != z))
-
-    def pass_weights(k):
+                go(
+                    remote(
+                        wp.at[par, y, cd, s],
+                        wb.at[z, y, cd, s],
+                        w_send.at[par, cd, s],
+                        w_recv.at[z, s],
+                        at(zt, cd),
+                    ),
+                    zt != z,
+                )
+
+    def pass_weights(k, s):
         for d in range(2):
             zs = from_there(d, k)
-            pl.when(has(d, k))(lambda zs=zs: weight_direct(zs).wait_recv())
-            go(weight_beside(zs), has(d, k))
-            go(weight_core(zs, 0), has(d, k))
+            pl.when(has(d, k))(lambda zs=zs: weight_direct(zs, s).wait_recv())
+            go(weight_beside(zs, y, s), has(d, k))
+            go(weight_core(zs, 0, c, s), has(d, k))
+
+    def pass_beside(k, s):
+        for d in range(2):
+            zs = from_there(d, k)
+            pl.when(has(d, k))(lambda zs=zs: weight_beside(zs, 1 - y, s).wait_recv())
+            go(weight_core(zs, 1, c, s), has(d, k))
 
     part = xg.shape[2] * xg.shape[3]
     tile = 2 * part
@@ -460,31 +453,26 @@
             values = rms_norm(values, norm_gain_ref[...])
             normed[i, h * part : (h + 1) * part, :] = values.astype(BF16)
 
-    pass_on(1)
-    send_weights()
-    pass_on(2)
-    pass_weights(1)
-    pass_weights(2)
-    own_x.wait()
+    others = [lax.rem(z + k, n) for k in range(1, n)]
+    pl.when(owner)(own_local.start)
+    go(own, owner)
+    for p in range(pieces):
+        send_weights(p)
+    for p in range(pieces):
+        pass_on(1, p)
+    for p in range(pieces):
+        for k in range(1, n):
+            pass_weights(k, p)
+        if p:
+            pass_on(2, p - 1)
+    pass_on(2, pieces - 1)
     norm_of(z)
-    pass_on(3)
-    pass_weights(3)
-    others = [lax.rem(z + k, n) for k in range(1, n)]
-    for k in range(1, n):
-        for d in range(2):
-            zs = from_there(d, k)
-
-            @pl.when(has(d, k))
-            def _(zs=zs):
-                remote(
-                    wb.at[zs, 1 - y, c],
-                    wb.at[zs, 1 - y, c],
-                    wy_send.at[zs],
-                    wy_recv.at[zs],
-                    beside,
-                ).wait_recv()
-
-            go(weight_core(zs, 1), has(d, k))
+    for p in range(pieces):
+        pass_on(3, p)
+    for p in range(pieces):
+        for k in range(1, n):
+            pass_beside(k, p)
+
     for k in range(1, n):
         for d in range(2):
 
@@ -504,17 +492,11 @@
     pl.when(jnp.logical_not(owner))(own.wait_recv)
     for zs in others:
         for which in range(2):
-            yy = y if which == 0 else 1 - y
-            remote(
-                wb.at[zs, yy, 1 - c],
-                wb.at[zs, yy, 1 - c],
-                wc_send.at[which, zs],
-                wc_recv.at[which, zs],
-                peer,
-            ).wait_recv()
-
-    depth = wb.shape[1] * wb.shape[2] * wb.shape[3]
-    width = wb.shape[4]
+            for p in range(pieces):
+                weight_core(zs, which, 1 - c, p).wait_recv()
+
+    depth = wb.shape[1] * wb.shape[2] * wb.shape[3] * wb.shape[4]
+    width = wb.shape[5]
     for i in range(n):
         acc = dot(normed[i, :, 0:depth], wb[0].reshape(depth, width))
         for j in range(1, n):
@@ -710,7 +692,7 @@
     piece = depth // 4
 
     def cut(weight):
-        return weight.reshape(2, CORES, piece, weight.shape[1])
+        return weight.reshape(2, CORES, pieces, piece // pieces, weight.shape[1])
 
     def line(vector):
         return vector.reshape(1, -1)
@@ -729,10 +711,10 @@
         scratch_shapes=[
             pltpu.VMEM(da_out_weight.shape, BF16),
             pltpu.VMEM(sw_out_weight.shape, BF16),
-            pltpu.VMEM((CORES, 2, CORES, piece, wide), BF16),
+            pltpu.VMEM((CORES, 2, CORES, pieces, piece // pieces, width), BF16),
             pltpu.VMEM((8, wide), F32),
             pltpu.VMEM((n, 2, pieces, part // pieces, d), BF16),
-            pltpu.VMEM((n, 2, CORES, piece, width), BF16),
+            pltpu.VMEM((n, 2, CORES, pieces, piece // pieces, width), BF16),
             pltpu.VMEM((n, tile, d), BF16),
             pltpu.VMEM((n, tile, 2 * wide), BF16),
             pltpu.VMEM((2, n, tile, 3 * wide), BF16),
@@ -743,17 +725,17 @@
             pltpu.VMEM((tile, d), BF16),
             pltpu.VMEM((tile, d), BF16),
             pltpu.VMEM((tile, d), BF16),
-            DMA((6,)),
+            DMA((14,)),
             DMA((2, n, pieces)),
             DMA((2, n, pieces)),
             DMA((n, pieces)),
             DMA((n, pieces)),
-            DMA((CORES, CORES)),
-            DMA((n,)),
-            DMA((n,)),
-            DMA((n,)),
-            DMA((2, n)),
-            DMA((2, n)),
+            DMA((CORES, CORES, pieces)),
+            DMA((n, pieces)),
+            DMA((n, pieces)),
+            DMA((n, pieces)),
+            DMA((2, n, pieces)),
+            DMA((2, n, pieces)),
             DMA,
             DMA,
             DMA,

time: 78.1 us -> 74.3 us (0.951); the launches traced: 76.8 us -> 74.1 us
  Pallas kernels: 74.5 us -> 71.8 us
    pallas_call x1, Pallas kernels: 74.5 us -> 71.8 us  [transposed(): pl.pallas_call(functools.partial(kernel, n), out_shape=jax.ShapeDtypeStru...]
where the time goes in v3:
time: 74.3 us; the launch traced here: 74.1 us
  Pallas kernels  71.8 us (97%)
  local copies, waits for them, and re-layouts  2.3 us (3%)
    pallas_call x1, Pallas kernels, transposed(): pl.pallas_call(functools.partial(kernel, n), out_shape=jax.ShapeDtypeStru...  71.8 us
    unnamed x1, local copies, waits for them, and re-layouts  2.3 us

profile of v3, /device:TPU:1, one launch (start us, length us, event | category | flops | bytes accessed | tf_op | source)
XLA Modules:
  0.0 74.1 jit_solution(11978768541310652418)
XLA Ops:
  0.0 71.8 %shard_map.163 = bf16[2,128,2048]{2,1,0:T(8,128)(2,1)} custom-call(bf16[2,2,4,16,2048]{4,3,2,1,0:T(8,128)(2,1)} %bitcast.17, bf16[2,2,4,32,256]{4,3,2,1,0:T(8,128)(2,1)} %bitcast.18, bf16[2,2,4,32,256]{4,3,2,1,0:T(8,128)(2,1)} %bitcast.19, bf16[2,2,4,32,256]{4,3,2,1,0:T(8,128)(2,1)} %bitcast.20, bf16[2,2,4,32,256]{4,3,2,1,0:T(8,128)(2,1)} %bitcast.21, ...), custom_call_target="tpu_custom_call" | custom-call | tf_op jit(solution)/shard_map/pallas_call | solution.py:706
  71.8 2.3 %copy.19 = bf16[256,2048]{1,0:T(8,128)(2,1)} copy(bf16[256,2048]{1,0:T(8,128)(2,1)} %bitcast.16) | data formatting | bytes 2097152

commit v4 on v3

--- a/solution.py
+++ b/solution.py
@@ -631,18 +631,23 @@
     for load in out_loads:
         load.wait()
     await_rows(1 - c)
-    for q in range(4):
-        part_out[:, q * columns : (q + 1) * columns] = project(1 - c, q)
-        cols = pl.ds(q * columns, columns)
-        go(remote(part_out.at[:, cols], part_in.at[:, cols], p_send.at[q], p_recv.at[q], peer))
-    await_rows(c)
-    for q in range(4):
-        cols = pl.ds(q * columns, columns)
-        mine_part = project(c, q).astype(F32)
-        remote(part_out.at[:, cols], part_in.at[:, cols], p_send.at[q], p_recv.at[q], peer).wait_recv()
+    for q in range(4 + 1):
+        if q < 4:
+            part_out[:, q * columns : (q + 1) * columns] = project(1 - c, q)
+            cols = pl.ds(q * columns, columns)
+            go(remote(part_out.at[:, cols], part_in.at[:, cols], p_send.at[q], p_recv.at[q], peer))
+        if q == 0:
+            await_rows(c)
+            continue
+        last = q - 1
+        cols = pl.ds(last * columns, columns)
+        mine_part = project(c, last).astype(F32)
+        remote(
+            part_out.at[:, cols], part_in.at[:, cols], p_send.at[last], p_recv.at[last], peer
+        ).wait_recv()
         both = mine_part + part_in[:, cols].astype(F32)
         sum_out[:, cols] = both.astype(BF16)
-        go(remote(sum_out.at[:, cols], sum_in.at[:, cols], s_send.at[q], s_recv.at[q], across))
+        go(remote(sum_out.at[:, cols], sum_in.at[:, cols], s_send.at[last], s_recv.at[last], across))
     for q in range(4):
         cols = pl.ds(q * columns, columns)
         remote(sum_out.at[:, cols], sum_in.at[:, cols], s_send.at[q], s_recv.at[q], across).wait_recv()

time: 74.3 us -> 73.7 us (level)
  no operation moved by 1% of the time
where the time goes in v4:
time: 73.7 us; the launch traced here: 73.5 us
  Pallas kernels  71.2 us (97%)
  local copies, waits for them, and re-layouts  2.3 us (3%)
    pallas_call x1, Pallas kernels, transposed(): pl.pallas_call(functools.partial(kernel, n), out_shape=jax.ShapeDtypeStru...  71.2 us
    unnamed x1, local copies, waits for them, and re-layouts  2.3 us

profile of v4, /device:TPU:1, one launch (start us, length us, event | category | flops | bytes accessed | tf_op | source)
XLA Modules:
  0.0 73.5 jit_solution(153374214071327091)
XLA Ops:
  0.0 71.2 %shard_map.163 = bf16[2,128,2048]{2,1,0:T(8,128)(2,1)} custom-call(bf16[2,2,4,16,2048]{4,3,2,1,0:T(8,128)(2,1)} %bitcast.17, bf16[2,2,4,32,256]{4,3,2,1,0:T(8,128)(2,1)} %bitcast.18, bf16[2,2,4,32,256]{4,3,2,1,0:T(8,128)(2,1)} %bitcast.19, bf16[2,2,4,32,256]{4,3,2,1,0:T(8,128)(2,1)} %bitcast.20, bf16[2,2,4,32,256]{4,3,2,1,0:T(8,128)(2,1)} %bitcast.21, ...), custom_call_target="tpu_custom_call" | custom-call | tf_op jit(solution)/shard_map/pallas_call | solution.py:711
  71.2 2.3 %copy.19 = bf16[256,2048]{1,0:T(8,128)(2,1)} copy(bf16[256,2048]{1,0:T(8,128)(2,1)} %bitcast.16) | data formatting | bytes 2097152
